TPU v7x, 32 devices: a whole 2x2x4 slice. The times are simulated.
32 devices in a mesh: rep: 4 (over y, x), fs: 2 (over core), tp: 4 (over z).
Axes of the slice: x: 2, y: 2, z: 4, core: 2. Of those that a mesh axis runs over, the one named last changes fastest.
Arguments:
- layer_input: bfloat16 [10240, 2048], P(('rep', 'fs'), 'tp'), may hold values from -6 to 6
- cotangent: bfloat16 [10240, 2048], P(('rep', 'fs'), 'tp'), may hold values from -8 to 8
- gate_pre: bfloat16 [10240, 3072], P('rep', 'fs'), may hold values from -8 to 8
- up_pre: bfloat16 [10240, 3072], P('rep', 'fs'), may hold values from -6 to 6
- gate_weight: bfloat16 [2048, 3072], P('tp', 'fs'), may hold values from -0.125 to 0.125
- up_weight: bfloat16 [2048, 3072], P('tp', 'fs'), may hold values from -0.125 to 0.125
- down_weight: bfloat16 [3072, 2048], P('fs', 'tp'), may hold values from -0.109375 to 0.109375
Outputs:
- input_grad: bfloat16 [10240, 2048], P(('rep', 'fs'), 'tp')
- gate_grad: float32 [2048, 3072], P('tp', 'fs')
- up_grad: float32 [2048, 3072], P('tp', 'fs')
- down_grad: float32 [3072, 2048], P('fs', 'tp')
- gate_rows_sq: float32 [2048], P('tp')
- up_rows_sq: float32 [2048], P('tp')
- down_rows_sq: float32 [3072], P('fs')
All inputs are finite; a program needn't handle non-finite values.
Results may differ from a plain program's by a relative error of at most 0.019.
Values may be sent and summed in bfloat16 or wider, within the bound.
No kernel may reach another device: no remote copies, remote signals or barrier semaphores. Data moves between devices by JAX's collectives and lax.ppermute only.
A program may use at most 128 MiB of HBM per device.

v0:
```python
import math
import jax
import jax.numpy as jnp
from jax import lax
from jax.sharding import PartitionSpec as P


def contract_rows(left_side, right_side):
    return lax.dot_general(
        left_side, right_side, (((0,), (0,)), ((), ())), preferred_element_type=jnp.float32
    )


def contract_cols(left_side, right_side):
    return lax.dot_general(
        left_side, right_side, (((1,), (1,)), ((), ())), preferred_element_type=jnp.float32
    )


def row_squares(gate_grad, up_grad, down_grad):
    gate_sq = jnp.sum(gate_grad * gate_grad, axis=1)
    up_sq = jnp.sum(up_grad * up_grad, axis=1)
    down_sq = jnp.sum(down_grad * down_grad, axis=1)
    gate_sq, up_sq = lax.psum((gate_sq, up_sq), "fs")
    down_sq = lax.psum(down_sq, "tp")
    return (gate_sq, up_sq, down_sq)


def on_device(layer_input, cotangent, gate_pre, up_pre, gate_weight, up_weight, down_weight):
    group_input, group_cotangent = (
        lax.all_gather(layer_input, "fs", axis=0, tiled=True),
        lax.all_gather(cotangent, "fs", axis=0, tiled=True),
    )
    hidden_grad = lax.psum(
        contract_cols(group_cotangent, down_weight).astype(jnp.bfloat16), "tp"
    ).astype(jnp.float32)
    gate_value = gate_pre.astype(jnp.float32)
    up_value = up_pre.astype(jnp.float32)
    sigmoid_gate = jax.nn.sigmoid(gate_value)
    activated = gate_value * sigmoid_gate
    hidden = (activated * up_value).astype(jnp.bfloat16)
    gate_delta = (
        hidden_grad * up_value * sigmoid_gate * (1.0 + gate_value * (1.0 - sigmoid_gate))
    ).astype(jnp.bfloat16)
    up_delta = (hidden_grad * activated).astype(jnp.bfloat16)
    input_grad = lax.psum_scatter(
        (contract_cols(gate_delta, gate_weight) + contract_cols(up_delta, up_weight)).astype(
            jnp.bfloat16
        ),
        "fs",
        scatter_dimension=0,
        tiled=True,
    )
    grad_scale = 1.0 / math.sqrt(group_input.shape[0] * lax.axis_size("rep"))
    gate_grad = contract_rows(group_input, gate_delta) * grad_scale
    up_grad = contract_rows(group_input, up_delta) * grad_scale
    down_grad = contract_rows(hidden, group_cotangent) * grad_scale
    gate_grad, up_grad, down_grad = (
        lax.psum(gate_grad.astype(jnp.bfloat16), "rep").astype(jnp.float32),
        lax.psum(up_grad.astype(jnp.bfloat16), "rep").astype(jnp.float32),
        lax.psum(down_grad.astype(jnp.bfloat16), "rep").astype(jnp.float32),
    )
    gate_sq, up_sq, down_sq = row_squares(gate_grad, up_grad, down_grad)
    return (input_grad, gate_grad, up_grad, down_grad, gate_sq, up_sq, down_sq)


def solution(mesh):
    return jax.shard_map(
        on_device,
        mesh=mesh,
        in_specs=(
            P(("rep", "fs"), "tp"),
            P(("rep", "fs"), "tp"),
            P("rep", "fs"),
            P("rep", "fs"),
            P("tp", "fs"),
            P("tp", "fs"),
            P("fs", "tp"),
        ),
        out_specs=(
            P(("rep", "fs"), "tp"),
            P("tp", "fs"),
            P("tp", "fs"),
            P("fs", "tp"),
            P("tp"),
            P("tp"),
            P("fs"),
        ),
        check_vma=False,
    )
```

profile of v0, /device:TPU:0, one launch (start us, length us, event | category | flops | bytes accessed | tf_op | source)
XLA Modules:
  0.0 484.3 jit_solution(10853355649280223357)
XLA Ops:
  7.2 0.0 copy-start
  7.2 0.0 all-gather.3.cloned.1.call-start
  7.2 0.7 all-gather.3.cloned.1.call-update
  7.9 0.0 all-reduce.5.cloned.1.call-start
  8.0 15.7 %all-gather.3.cloned.1.call-done = bf16[2560,512]{1,0:T(8,128)(2,1)} async-done(((bf16[1280,512]{1,0:T(8,128)(2,1)}), bf16[2560,512]{1,0:T(8,128)(2,1)}) %all-gather.3.cloned.1.call-update) | async-done | bytes 2621456 | tf_op jit(solution)/shard_map/all_gather | solution.py:32
  23.6 0.0 copy-done
  23.6 8.2 %convolution_convert_fusion = bf16[2560,1536]{1,0:T(8,128)(2,1)} fusion(bf16[2560,512]{1,0:T(8,128)(2,1)} %all-gather.3.cloned.1.call-done, bf16[1536,512]{1,0:T(8,128)(2,1)S(1)} %copy-done), kind=kOutput, calls=%fused_computation.15 | convolution fusion | flops 4030464000 | bytes 12058624 | tf_op jit(solution)/shard_map/dot_general | solution.py:15
  31.9 0.0 all-reduce.5.cloned.1.call-update
  31.9 0.0 all-gather.5.cloned.1.call-start
  32.0 0.7 all-gather.5.cloned.1.call-update
  32.6 0.0 all-reduce.7.cloned.1.call-start
  32.7 10.0 %fusion.14 = bf16[1536,512]{1,0:T(8,128)(2,1)} fusion(bf16[2560,512]{1,0:T(8,128)(2,1)} %all-gather.3.cloned.1.call-done, bf16[2560,1536]{1,0:T(8,128)(2,1)} %param.10, bf16[2560,1536]{1,0:T(8,128)(2,1)} %param.9), kind=kOutput, calls=%fused_computation.24 | convolution fusion | flops 4059561984 | bytes 19922944 | tf_op jit(solution)/shard_map/dot_general | solution.py:9
  42.7 264.3 %all-reduce.5.cloned.1.call-done = bf16[2560,1536]{1,0:T(8,128)(2,1)} async-done(((bf16[2560,1536]{1,0:T(8,128)(2,1)}), bf16[2560,1536]{1,0:T(8,128)(2,1)}) %all-reduce.5.cloned.1.call-update) | async-done | bytes 7864336 | tf_op jit(solution)/shard_map/psum | solution.py:34
  307.0 17.0 %fusion = (bf16[2560,1536]{1,0:T(8,128)(2,1)}, bf16[2560,1536]{1,0:T(8,128)(2,1)}) fusion(bf16[2560,1536]{1,0:T(8,128)(2,1)} %all-reduce.5.cloned.1.call-done, bf16[2560,1536]{1,0:T(8,128)(2,1)} %param.9, bf16[2560,1536]{1,0:T(8,128)(2,1)} %param.10), kind=kLoop, calls=%fused_computation.6 | loop fusion | flops 62914560 | bytes 39321600 | tf_op jit(solution)/shard_map/convert_element_type | solution.py:45
  324.1 9.6 %fusion.20 = bf16[512,1536]{0,1:T(8,128)(2,1)} fusion(bf16[2560,1536]{1,0:T(8,128)(2,1)} %get-tuple-element.22, bf16[2560,512]{1,0:T(8,128)(2,1)} %all-gather.5.cloned.1.call-done), kind=kOutput, calls=%fused_computation.28 | convolution fusion | flops 4028104704 | bytes 12058624 | tf_op jit(solution)/shard_map/dot_general | solution.py:9
  333.6 0.0 copy-done.2
  333.6 0.0 copy-done.4
  333.6 5.4 %fusion.19 = bf16[512,1536]{0,1:T(8,128)(2,1)} fusion(bf16[2560,1536]{1,0:T(8,128)(2,1)S(1)} %copy-done.2, bf16[2560,512]{1,0:T(8,128)(2,1)S(1)} %copy-done.4), kind=kOutput, calls=%fused_computation.27 | convolution fusion | flops 4028104704 | bytes 12058624 | tf_op jit(solution)/shard_map/dot_general | solution.py:9
  339.0 0.0 all-reduce.7.cloned.1.call-update
  339.0 0.0 copy-start.6
  339.0 0.2 reduce-scatter.2.cloned.1.call-start
  339.3 0.0 copy-done.5
  339.3 6.9 %fusion.22 = f32[2560,512]{1,0:T(8,128)S(1)} fusion(bf16[2560,1536]{1,0:T(8,128)(2,1)} %get-tuple-element.22, bf16[512,1536]{1,0:T(8,128)(2,1)S(1)} %copy-done.5), kind=kOutput, calls=%fused_computation.30 | convolution fusion | flops 4026531840 | bytes 14680064 | tf_op jit(solution)/shard_map/dot_general | solution.py:15
  346.2 9.2 %add_convert_fusion = bf16[2560,512]{1,0:T(8,128)(2,1)} fusion(f32[2560,512]{1,0:T(8,128)S(1)} %fusion.22, bf16[2560,1536]{1,0:T(8,128)(2,1)} %get-tuple-element.21, bf16[512,1536]{1,0:T(8,128)(2,1)S(1)} %copy-done.6), kind=kOutput, calls=%fused_computation.17 | convolution fusion | flops 4029153280 | bytes 17301504 | tf_op jit(solution)/shard_map/dot_general | solution.py:15
  355.4 0.0 reduce-scatter.2.cloned.1.call-update
  355.4 94.9 %all-reduce.7.cloned.1.call-done = (bf16[512,1536]{0,1:T(8,128)(2,1)}, bf16[512,1536]{0,1:T(8,128)(2,1)}, bf16[1536,512]{1,0:T(8,128)(2,1)}) async-done(((bf16[512,1536]{0,1:T(8,128)(2,1)}, bf16[512,1536]{0,1:T(8,128)(2,1)}, bf16[1536,512]{1,0:T(8,128)(2,1)}), (bf16[512,1536]{0,1:T(8,128)(2,1)}, bf16[512,1536]{0,1:T(8,128)(2,1)}, bf16[1536,512]{1,0:T(8,128)(2,1)})) %all-reduce.7.cloned.1.call-update) | async-done | bytes 4718608 | tf_op jit(solution)/shard_map/psum | solution.py:59
  450.4 3.2 copy.14
  453.5 3.2 copy.15
  456.7 2.1 multiply_reduce_fusion.1
  458.8 3.0 all-reduce
  461.8 3.5 multiply_reduce_fusion
  465.3 12.4 %psum.55 = f32[1536]{0:T(1024)} all-reduce(f32[1536]{0:T(1024)S(1)} %get-tuple-element.19), channel_id=1, replica_groups=mesh['rep'=4,'fs'=2,'tp'=4] {'tp'}, use_global_device_ids=true, to_apply=%region_10.0 | all-reduce | flops 1536 | bytes 12288 | tf_op jit(solution)/shard_map/psum | solution.py:25
  (10 shorter events, 0.0 us)
Async XLA Ops:
  7.2 16.5 %copy-start = (bf16[1536,512]{1,0:T(8,128)(2,1)S(1)}, bf16[1536,512]{1,0:T(8,128)(2,1)}, u32[]{:S(2)}) copy-start(bf16[1536,512]{1,0:T(8,128)(2,1)} %param.13) | copy-start | bytes 4718596
  7.2 16.5 %all-gather.3.cloned.1.call-start = ((), (), s32[]{:S(2)}) async-start(), calls=%async_computation.1 | async-start | bytes 3932160 | tf_op jit(solution)/shard_map/all_gather | solution.py:32
  7.9 299.1 %all-reduce.5.cloned.1.call-start = ((), (), s32[]{:S(2)}) async-start(), calls=%async_computation.2 | async-start | bytes 15728640 | tf_op jit(solution)/shard_map/psum | solution.py:34
  31.9 292.1 %all-gather.5.cloned.1.call-start = ((), (), s32[]{:S(2)}) async-start(), calls=%async_computation.4 | async-start | bytes 3932160 | tf_op jit(solution)/shard_map/all_gather | solution.py:31
  32.6 417.7 %all-reduce.7.cloned.1.call-start = ((), (), s32[]{:S(2)}) async-start(), calls=%async_computation.5 | async-start | bytes 9437184 | tf_op jit(solution)/shard_map/psum | solution.py:59
  324.1 9.6 %copy-start.2 = (bf16[2560,1536]{1,0:T(8,128)(2,1)S(1)}, bf16[2560,1536]{1,0:T(8,128)(2,1)}, u32[]{:S(2)}) copy-start(bf16[2560,1536]{1,0:T(8,128)(2,1)} %get-tuple-element.21) | copy-start | bytes 23592964
  324.1 9.6 %copy-start.4 = (bf16[2560,512]{1,0:T(8,128)(2,1)S(1)}, bf16[2560,512]{1,0:T(8,128)(2,1)}, u32[]{:S(2)}) copy-start(bf16[2560,512]{1,0:T(8,128)(2,1)} %all-gather.5.cloned.1.call-done) | copy-start | bytes 7864324
  333.6 5.7 %copy-start.5 = (bf16[512,1536]{1,0:T(8,128)(2,1)S(1)}, bf16[512,1536]{1,0:T(8,128)(2,1)}, u32[]{:S(2)}) copy-start(bf16[512,1536]{1,0:T(8,128)(2,1)} %param.11) | copy-start | bytes 4718596
  339.0 7.1 %copy-start.6 = (bf16[512,1536]{1,0:T(8,128)(2,1)S(1)}, bf16[512,1536]{1,0:T(8,128)(2,1)}, u32[]{:S(2)}) copy-start(bf16[512,1536]{1,0:T(8,128)(2,1)} %param.12) | copy-start | bytes 4718596
  339.0 138.7 %reduce-scatter.2.cloned.1.call-start = ((), (), s32[]{:S(2)}) async-start(), calls=%async_computation.3 | async-start | bytes 3932160 | tf_op jit(solution)/shard_map/reduce_scatter | solution.py:46
  450.3 6.4 %copy-start.3 = (bf16[512,1536]{0,1:T(8,128)(2,1)S(1)}, bf16[512,1536]{0,1:T(8,128)(2,1)}, u32[]{:S(2)}) copy-start(bf16[512,1536]{0,1:T(8,128)(2,1)} %get-tuple-element.16) | copy-start | bytes 4718596
  453.5 24.2 %copy-start.1 = (bf16[1536,512]{1,0:T(8,128)(2,1)S(1)}, bf16[1536,512]{1,0:T(8,128)(2,1)}, u32[]{:S(2)}) copy-start(bf16[1536,512]{1,0:T(8,128)(2,1)} %param.13) | copy-start | bytes 4718596
Sparse Core Ops, SparseCore 0:
  9.5 14.0 all-gather.2
  32.0 274.9 all-reduce.4
  308.6 10.1 all-gather.4
  339.2 111.1 all-reduce.6
  453.0 10.4 reduce-scatter.1
where the time goes:
time: 485 us; the launch traced here: 484 us
  waiting for transfers between devices  376 us (78%)
  matrix products  49.3 us (10%)
  other arithmetic  22.6 us (5%)
  blocking collectives  15.4 us (3%)
  between operations  13.8 us (3%)
  local copies, waits for them, and re-layouts  6.41 us (1%)
    psum x1, waiting for transfers between devices, on_device(): lax.psum(contract_cols(group_cotangent, down_weight).astype(jnp.bfloat16)...  264 us
    psum x1, waiting for transfers between devices, on_device(): lax.psum(gate_grad.astype(jnp.bfloat16), 'rep').astype(jnp.float32)  94.9 us
    dot_general x3, matrix products, contract_rows(): lax.dot_general(left_side, right_side, (((0,), (0,)), ((), ())), preferre...  25 us
    dot_general x3, matrix products, contract_cols(): lax.dot_general(left_side, right_side, (((1,), (1,)), ((), ())), preferre...  24.3 us
    convert_element_type x1, other arithmetic, on_device(): up_delta = (hidden_grad * activated).astype(jnp.bfloat16)  17 us
    all_gather x1, waiting for transfers between devices, on_device(): lax.all_gather(cotangent, 'fs', axis=0, tiled=True)  15.7 us
    psum x1, blocking collectives, row_squares(): down_sq = lax.psum(down_sq, 'tp')  12.4 us
  transfers between devices with their start and end apart: 5, of which 3 were waited for; matrix products, arithmetic and copies ran while one was open for 11% of the time, Pallas kernels for 0%

commit v1 on v0

--- a/solution.py
+++ b/solution.py
@@ -56,7 +56,7 @@
     up_grad = contract_rows(group_input, up_delta) * grad_scale
     down_grad = contract_rows(hidden, group_cotangent) * grad_scale
     gate_grad, up_grad, down_grad = (
-        lax.psum(gate_grad.astype(jnp.bfloat16), "rep").astype(jnp.float32),
+        jnp.sum(lax.all_gather(gate_grad.astype(jnp.bfloat16), "rep"), axis=0).astype(jnp.float32),
         lax.psum(up_grad.astype(jnp.bfloat16), "rep").astype(jnp.float32),
         lax.psum(down_grad.astype(jnp.bfloat16), "rep").astype(jnp.float32),
     )

time: 485 us -> 526 us (1.085)
  waiting for transfers between devices: 376 us -> 396 us
  local copies, waits for them, and re-layouts: 6.41 us -> 16.6 us
  other arithmetic: 22.6 us -> 30.4 us
    all_gather x0 -> x1, waiting for transfers between devices: none -> 54.1 us  [on_device(): lax.all_gather(gate_grad.astype(jnp.bfloat16), 'rep')]
    psum x1, waiting for transfers between devices: 94.9 us -> 60 us  [on_device(): lax.psum(up_grad.astype(jnp.bfloat16), 'rep').astype(jnp.float32)]
    all_gather x0 -> x1, local copies, waits for them, and re-layouts: none -> 11.3 us  [on_device(): lax.all_gather(gate_grad.astype(jnp.bfloat16), 'rep')]
    reduce_sum x0 -> x2, other arithmetic: none -> 11 us  [the longest x1 10.6 us: on_device(): jnp.sum(lax.all_gather(gate_grad.astype(jnp.bfloat16), 'rep'), axis=0)]
  transfers between devices with their start and end apart: 5 -> 6, of which waited for: 3 -> 4; matrix products, arithmetic and copies ran while one was open for 11% -> 16% of each run, Pallas kernels for 0% -> 0%
where the time goes in v1:
time: 526 us
  waiting for transfers between devices  396 us (75%)
  matrix products  53.2 us (10%)
  other arithmetic  30.4 us (6%)
  local copies, waits for them, and re-layouts  16.6 us (3%)
  blocking collectives  15.5 us (3%)
  between operations  14.2 us (3%)
    psum x1, waiting for transfers between devices, on_device(): lax.psum(contract_cols(group_cotangent, down_weight).astype(jnp.bfloat16)...  264 us
    psum x1, waiting for transfers between devices, on_device(): lax.psum(up_grad.astype(jnp.bfloat16), 'rep').astype(jnp.float32)  60 us
    all_gather x1, waiting for transfers between devices, on_device(): lax.all_gather(gate_grad.astype(jnp.bfloat16), 'rep')  54.1 us
    dot_general x3, matrix products, contract_rows(): lax.dot_general(left_side, right_side, (((0,), (0,)), ((), ())), preferre...  29 us
    dot_general x3, matrix products, contract_cols(): lax.dot_general(left_side, right_side, (((1,), (1,)), ((), ())), preferre...  24.2 us
    convert_element_type x1, other arithmetic, on_device(): up_delta = (hidden_grad * activated).astype(jnp.bfloat16)  17 us
    all_gather x1, waiting for transfers between devices, on_device(): lax.all_gather(cotangent, 'fs', axis=0, tiled=True)  15.7 us
    psum x1, blocking collectives, row_squares(): down_sq = lax.psum(down_sq, 'tp')  12.5 us
  transfers between devices with their start and end apart: 6, of which 4 were waited for; matrix products, arithmetic and copies ran while one was open for 16% of the time, Pallas kernels for 0%

profile of v1, /device:TPU:0, one launch (start us, length us, event | category | flops | bytes accessed | tf_op | source)
XLA Modules:
  0.0 525.8 jit_solution(13402343585880111398)
XLA Ops:
  7.2 0.0 all-gather.5.cloned.1.call-start
  7.2 0.7 all-gather.5.cloned.1.call-update
  7.9 0.0 all-reduce.5.cloned.1.call-start
  8.0 15.7 %all-gather.5.cloned.1.call-done = bf16[2560,512]{1,0:T(8,128)(2,1)} async-done(((bf16[1280,512]{1,0:T(8,128)(2,1)}), bf16[2560,512]{1,0:T(8,128)(2,1)}) %all-gather.5.cloned.1.call-update) | async-done | bytes 2621456 | tf_op jit(solution)/shard_map/all_gather | solution.py:32
  23.6 8.1 %convolution_convert_fusion = bf16[2560,1536]{1,0:T(8,128)(2,1)} fusion(bf16[2560,512]{1,0:T(8,128)(2,1)} %all-gather.5.cloned.1.call-done, bf16[1536,512]{1,0:T(8,128)(2,1)S(1)} %copy-done), kind=kOutput, calls=%fused_computation.15 | convolution fusion | flops 4030464000 | bytes 12058624 | tf_op jit(solution)/shard_map/dot_general | solution.py:15
  31.8 0.0 all-reduce.5.cloned.1.call-update
  31.8 0.0 all-gather.7.cloned.1.call-start
  31.9 0.7 all-gather.7.cloned.1.call-update
  32.5 0.0 all-reduce.7.cloned.1.call-start
  32.6 10.0 %fusion.14 = bf16[1536,512]{1,0:T(8,128)(2,1)} fusion(bf16[2560,512]{1,0:T(8,128)(2,1)} %all-gather.5.cloned.1.call-done, bf16[2560,1536]{1,0:T(8,128)(2,1)} %param.10, bf16[2560,1536]{1,0:T(8,128)(2,1)} %param.9), kind=kOutput, calls=%fused_computation.24 | convolution fusion | flops 4059561984 | bytes 19922944 | tf_op jit(solution)/shard_map/dot_general | solution.py:9
  42.6 264.3 %all-reduce.5.cloned.1.call-done = bf16[2560,1536]{1,0:T(8,128)(2,1)} async-done(((bf16[2560,1536]{1,0:T(8,128)(2,1)}), bf16[2560,1536]{1,0:T(8,128)(2,1)}) %all-reduce.5.cloned.1.call-update) | async-done | bytes 7864336 | tf_op jit(solution)/shard_map/psum | solution.py:34
  306.9 17.0 %fusion = (bf16[2560,1536]{1,0:T(8,128)(2,1)}, bf16[2560,1536]{1,0:T(8,128)(2,1)}) fusion(bf16[2560,1536]{1,0:T(8,128)(2,1)} %all-reduce.5.cloned.1.call-done, bf16[2560,1536]{1,0:T(8,128)(2,1)} %param.9, bf16[2560,1536]{1,0:T(8,128)(2,1)} %param.10), kind=kLoop, calls=%fused_computation.6 | loop fusion | flops 62914560 | bytes 39321600 | tf_op jit(solution)/shard_map/convert_element_type | solution.py:45
  324.0 9.4 %fusion.19 = bf16[512,1536]{0,1:T(8,128)(2,1)} fusion(bf16[2560,1536]{1,0:T(8,128)(2,1)} %get-tuple-element.27, bf16[2560,512]{1,0:T(8,128)(2,1)} %all-gather.7.cloned.1.call-done), kind=kOutput, calls=%fused_computation.27 | convolution fusion | flops 4028104704 | bytes 12058624 | tf_op jit(solution)/shard_map/dot_general | solution.py:9
  333.4 0.0 all-reduce.7.cloned.1.call-update
  333.4 0.2 all-gather.9.cloned.1.call-start
  333.6 9.5 %fusion.20 = bf16[512,1536]{0,1:T(8,128)(2,1)} fusion(bf16[2560,1536]{1,0:T(8,128)(2,1)} %get-tuple-element.28, bf16[2560,512]{1,0:T(8,128)(2,1)} %all-gather.7.cloned.1.call-done), kind=kOutput, calls=%fused_computation.28 | convolution fusion | flops 4028104704 | bytes 12058624 | tf_op jit(solution)/shard_map/dot_general | solution.py:9
  343.2 0.0 all-gather.9.cloned.1.call-update
  343.2 0.0 reduce-scatter.2.cloned.1.call-start
  343.3 6.8 %fusion.22 = f32[2560,512]{1,0:T(8,128)S(1)} fusion(bf16[2560,1536]{1,0:T(8,128)(2,1)} %get-tuple-element.28, bf16[512,1536]{1,0:T(8,128)(2,1)S(1)} %copy-done.4), kind=kOutput, calls=%fused_computation.30 | convolution fusion | flops 4026531840 | bytes 14680064 | tf_op jit(solution)/shard_map/dot_general | solution.py:15
  350.1 9.2 %add_convert_fusion = bf16[2560,512]{1,0:T(8,128)(2,1)} fusion(f32[2560,512]{1,0:T(8,128)S(1)} %fusion.22, bf16[2560,1536]{1,0:T(8,128)(2,1)} %get-tuple-element.27, bf16[512,1536]{1,0:T(8,128)(2,1)S(1)} %copy-done.5), kind=kOutput, calls=%fused_computation.17 | convolution fusion | flops 4029153280 | bytes 17301504 | tf_op jit(solution)/shard_map/dot_general | solution.py:15
  359.3 0.0 reduce-scatter.2.cloned.1.call-update
  359.4 60.0 %all-reduce.7.cloned.1.call-done = (bf16[512,1536]{0,1:T(8,128)(2,1)}, bf16[1536,512]{1,0:T(8,128)(2,1)}) async-done(((bf16[512,1536]{0,1:T(8,128)(2,1)}, bf16[1536,512]{1,0:T(8,128)(2,1)}), (bf16[512,1536]{0,1:T(8,128)(2,1)}, bf16[1536,512]{1,0:T(8,128)(2,1)})) %all-reduce.7.cloned.1.call-update) | async-done | bytes 3145744 | tf_op jit(solution)/shard_map/psum | solution.py:60
  419.4 3.2 copy.16
  422.6 2.0 multiply_reduce_fusion
  424.6 12.5 %psum.47 = f32[1536]{0:T(1024)} all-reduce(f32[1536]{0:T(1024)S(1)} %get-tuple-element.25), channel_id=1, replica_groups=mesh['rep'=4,'fs'=2,'tp'=4] {'tp'}, use_global_device_ids=true, to_apply=%region_10.0 | all-reduce | flops 1536 | bytes 12288 | tf_op jit(solution)/shard_map/psum | solution.py:25
  437.0 0.4 multiply_reduce_fusion.1
  437.4 54.1 %all-gather.9.cloned.1.call-done = bf16[2048,1536]{0,1:T(8,128)(2,1)} async-done(((bf16[512,1536]{0,1:T(8,128)(2,1)}), bf16[2048,1536]{0,1:T(8,128)(2,1)}) %all-gather.9.cloned.1.call-update) | async-done | bytes 6291472 | tf_op jit(solution)/shard_map/all_gather | solution.py:59
  491.5 11.3 %reshape.14 = bf16[4,512,1536]{1,0,2:T(4,128)(2,1)} reshape(bf16[2048,1536]{0,1:T(8,128)(2,1)} %all-gather.9.cloned.1.call-done) | data formatting | bytes 12582912 | tf_op jit(solution)/shard_map/all_gather | solution.py:59
  502.9 10.6 %reduce_sum.39 = bf16[512,1536]{0,1:T(8,128)(2,1)S(1)} reduce(bf16[4,512,1536]{1,0,2:T(4,128)(2,1)} %reshape.14, bf16[]{:T(256)} %constant.3.clone.1), dimensions={0}, to_apply=%region_2.0 | reduce | flops 2359296 | bytes 7864322 | tf_op jit(solution)/shard_map/reduce_sum | solution.py:59
  513.5 2.1 copy.15
  515.5 0.4 multiply_reduce_fusion.2
  515.9 3.0 all-reduce
  (14 shorter events, 0.0 us)
Async XLA Ops:
  7.2 16.5 %copy-start = (bf16[1536,512]{1,0:T(8,128)(2,1)S(1)}, bf16[1536,512]{1,0:T(8,128)(2,1)}, u32[]{:S(2)}) copy-start(bf16[1536,512]{1,0:T(8,128)(2,1)} %param.13) | copy-start | bytes 4718596
  7.2 16.5 %all-gather.5.cloned.1.call-start = ((), (), s32[]{:S(2)}) async-start(), calls=%async_computation.1 | async-start | bytes 3932160 | tf_op jit(solution)/shard_map/all_gather | solution.py:32
  7.9 299.0 %all-reduce.5.cloned.1.call-start = ((), (), s32[]{:S(2)}) async-start(), calls=%async_computation.2 | async-start | bytes 15728640 | tf_op jit(solution)/shard_map/psum | solution.py:34
  31.8 292.2 %all-gather.7.cloned.1.call-start = ((), (), s32[]{:S(2)}) async-start(), calls=%async_computation.4 | async-start | bytes 3932160 | tf_op jit(solution)/shard_map/all_gather | solution.py:31
  32.5 386.8 %all-reduce.7.cloned.1.call-start = ((), (), s32[]{:S(2)}) async-start(), calls=%async_computation.6 | async-start | bytes 6291456 | tf_op jit(solution)/shard_map/psum | solution.py:60
  333.4 158.2 %all-gather.9.cloned.1.call-start = ((), (), s32[]{:S(2)}) async-start(), calls=%async_computation.5 | async-start | bytes 7864320 | tf_op jit(solution)/shard_map/all_gather | solution.py:59
  333.6 9.6 %copy-start.4 = (bf16[512,1536]{1,0:T(8,128)(2,1)S(1)}, bf16[512,1536]{1,0:T(8,128)(2,1)}, u32[]{:S(2)}) copy-start(bf16[512,1536]{1,0:T(8,128)(2,1)} %param.11) | copy-start | bytes 4718596
  343.2 6.9 %copy-start.5 = (bf16[512,1536]{1,0:T(8,128)(2,1)S(1)}, bf16[512,1536]{1,0:T(8,128)(2,1)}, u32[]{:S(2)}) copy-start(bf16[512,1536]{1,0:T(8,128)(2,1)} %param.12) | copy-start | bytes 4718596
  343.2 175.8 %reduce-scatter.2.cloned.1.call-start = ((), (), s32[]{:S(2)}) async-start(), calls=%async_computation.3 | async-start | bytes 3932160 | tf_op jit(solution)/shard_map/reduce_scatter | solution.py:46
  419.4 3.2 copy-start.3
  419.4 17.7 %copy-start.2 = (bf16[512,1536]{0,1:T(8,128)(2,1)S(1)}, bf16[512,1536]{0,1:T(8,128)(2,1)}, u32[]{:S(2)}) copy-start(bf16[512,1536]{0,1:T(8,128)(2,1)} %get-tuple-element.23) | copy-start | bytes 4718596
  491.5 27.4 %copy-start.1 = (bf16[1536,512]{1,0:T(8,128)(2,1)S(1)}, bf16[1536,512]{1,0:T(8,128)(2,1)}, u32[]{:S(2)}) copy-start(bf16[1536,512]{1,0:T(8,128)(2,1)} %param.13) | copy-start | bytes 4718596
Sparse Core Ops, SparseCore 0:
  9.5 14.0 all-gather.4
  31.9 274.9 all-reduce.4
  308.5 10.1 all-gather.6
  333.5 85.8 all-reduce.6
  421.6 69.8 all-gather.8
  494.2 10.4 reduce-scatter.1
